TPU v7x, 32 devices: a whole 2x2x4 slice. The times are simulated.
32 devices in a mesh: sp: 8 (over z, x), dp: 4 (over y, core).
Axes of the slice: x: 2, y: 2, z: 4, core: 2. Of those that a mesh axis runs over, the one named last changes fastest.
Arguments:
- resid: bfloat16 [4, 1024, 2048], P('dp', 'sp'), may hold values from -6 to 6
- queries: bfloat16 [4, 1024, 2048], P('dp', 'sp'), may hold values from -7 to 7
- keys: bfloat16 [4, 1024, 2048], P('dp', 'sp'), may hold values from -7 to 7
- values: bfloat16 [4, 1024, 2048], P('dp', 'sp'), may hold values from -6 to 6
- forget_cache: float32 [4, 32, 1024], P('dp', 'sp'), may hold values from -131 to 0, as said below
- query_gain: float32 [64], replicated, may hold values from 0.5 to 8
- key_gain: float32 [64], replicated, may hold values from 0.5 to 8
- out_weight: bfloat16 [2048, 2048], P(None, 'dp'), may hold values from -0.125 to 0.125
- norm_gain: float32 [2048], replicated, may hold values from 0.1 to 1.9
- routes: int32 [4, 1024, 2], P('dp', 'sp'), may hold values from 0 to 31, all different within a row; in each aligned block of 128 rows (0 to 127, 128 to 255, ..., all dimensions but the last counted through in order) at most 16 rows name the same one
- group_weight: float32 [4, 1024], P('dp', 'sp'), may hold values from 0.2 to 1
- inner_share: float32 [4, 1024, 2], P('dp', 'sp'), may hold values from 0.1 to 1
- expert_gate: bfloat16 [32, 2048, 1024], P(('sp', 'dp')), may hold values from -0.125 to 0.125
- expert_up: bfloat16 [32, 2048, 1024], P(('sp', 'dp')), may hold values from -0.125 to 0.125
- expert_down: bfloat16 [32, 1024, 2048], P(('sp', 'dp')), may hold values from -0.1875 to 0.1875
Outputs:
- layer_out: bfloat16 [4, 1024, 2048], P('dp', 'sp')
Inputs may be any that keep to these rules, and one draw needn't show every extreme that they name: `routes`: each row names 2 different experts; the rows of one device name one expert at most 16 times, a bound that some block reaches. `forget_cache`: along positions each head's values never rise.
All inputs are finite; a program needn't handle non-finite values.
Results may differ from a plain program's by a relative error of at most 0.0095.
The roundings to bfloat16 on the way count: a program that leaves them out, or rounds other values in their place, can miss the bound.
Values may be sent and summed in bfloat16 or wider, within the bound.
A program may use at most 128 MiB of HBM per device.

v0:
```python
import functools

import jax
import jax.numpy as jnp
from jax import lax
from jax.experimental import pallas as pl
from jax.experimental.pallas import tpu as pltpu
from jax.sharding import PartitionSpec as P

EPS = 1e-06


def norm_rows(inputs, gain):
    floats = inputs.astype(jnp.float32)
    scaled = floats * lax.rsqrt(jnp.mean(floats * floats, axis=-1, keepdims=True) + EPS)
    return (scaled * gain).astype(jnp.bfloat16)


MESH = pl.DeviceIdType.MESH
LANES = 128
BLOCK = 256


def place(index, size):
    return pl.ds(pl.multiple_of(index * size, size), size)


def half_means(squares, head_size):
    lane = lax.broadcasted_iota(jnp.int32, (LANES, LANES), 0) // head_size
    other = lax.broadcasted_iota(jnp.int32, (LANES, LANES), 1) // head_size
    same = (lane == other).astype(jnp.float32).astype(jnp.bfloat16)
    high = squares.astype(jnp.bfloat16)
    low = (squares - high.astype(jnp.float32)).astype(jnp.bfloat16)
    total = jnp.dot(high, same, preferred_element_type=jnp.float32)
    total = total + jnp.dot(low, same, preferred_element_type=jnp.float32)
    return total * (1.0 / head_size)


def attention_kernel(
    n, head_size,
    q_ref, k_ref, v_ref, decay_ref, q_gain_ref, k_gain_ref,
    out_ref,
    q_buf, k_buf, v_buf, q_norm, k_head, v_ones, o_buf,
    local_sem, send_sem, recv_sem, own_sem, back_send, back_recv,
):
    me = lax.axis_index("sp")
    tok = q_ref.shape[0]
    pairs, length = q_buf.shape[0], q_buf.shape[1]
    inner = LANES // head_size
    sources, buffers = (q_ref, k_ref, v_ref), (q_buf, k_buf, v_buf)

    barrier = pltpu.get_barrier_semaphore()
    for step in range(1, n):
        pl.semaphore_signal(
            barrier, inc=1, device_id={"sp": lax.rem(me + step, n)}, device_id_type=MESH
        )
    pl.semaphore_wait(barrier, n - 1)

    def outgoing(kind, pair, step):
        target = lax.rem(me + step, n)
        return pltpu.make_async_remote_copy(
            src_ref=sources[kind].at[:, place(target * pairs + pair, LANES)],
            dst_ref=buffers[kind].at[pair, place(me, tok), :],
            send_sem=send_sem.at[kind, pair, step],
            recv_sem=recv_sem.at[kind, pair, step],
            device_id={"sp": target},
            device_id_type=MESH,
        )

    def own(kind, pair):
        return pltpu.make_async_copy(
            sources[kind].at[:, place(me * pairs + pair, LANES)],
            buffers[kind].at[pair, place(me, tok), :],
            local_sem.at[kind, pair],
        )

    def backward(pair, step):
        target = lax.rem(me + step, n)
        return pltpu.make_async_remote_copy(
            src_ref=o_buf.at[pair, place(target, tok), :],
            dst_ref=out_ref.at[:, place(me * pairs + pair, LANES)],
            send_sem=back_send.at[pair, step],
            recv_sem=back_recv.at[pair, step],
            device_id={"sp": target},
            device_id_type=MESH,
        )

    def own_back(pair):
        return pltpu.make_async_copy(
            o_buf.at[pair, place(me, tok), :],
            out_ref.at[:, place(me * pairs + pair, LANES)],
            own_sem.at[pair],
        )

    for pair in range(pairs):
        for step in range(1, n):
            for kind in range(3):
                outgoing(kind, pair, step).start()
        for kind in range(3):
            own(kind, pair).start()

    row = lax.broadcasted_iota(jnp.int32, (BLOCK, BLOCK), 0)
    col = lax.broadcasted_iota(jnp.int32, (BLOCK, BLOCK), 1)
    lane = lax.broadcasted_iota(jnp.int32, (length, LANES), 1) // head_size
    out_lane = lax.broadcasted_iota(jnp.int32, (BLOCK, LANES), 1) // head_size
    scale = head_size ** (-0.5)
    v_ones[:, LANES:] = jnp.ones((length, LANES), jnp.bfloat16)

    def scores_of(queries, keys):
        return lax.dot_general(
            queries, keys, (((1,), (1,)), ((), ())), preferred_element_type=jnp.float32
        )

    def one_pair(pair, carry):
        for kind in range(3):
            own(kind, pair).wait()
            for step in range(1, n):
                outgoing(kind, pair, step).wait_recv()
        floats = q_buf[pair].astype(jnp.float32)
        floats = floats * lax.rsqrt(half_means(floats * floats, head_size) + EPS)
        normed = (floats * q_gain_ref[...]).astype(jnp.bfloat16)
        q_norm[...] = (normed.astype(jnp.float32) * scale).astype(jnp.bfloat16)
        floats = k_buf[pair].astype(jnp.float32)
        floats = floats * lax.rsqrt(half_means(floats * floats, head_size) + EPS)
        floats = floats * k_gain_ref[...]
        for head in range(inner):
            k_head[head] = jnp.where(lane == head, floats, 0.0).astype(jnp.bfloat16)
        v_ones[:, :LANES] = v_buf[pair]
        for block in range(length // BLOCK):
            first = block * BLOCK
            here = slice(first, first + BLOCK)
            query_block = q_norm[here, :]
            merged = None
            for head in range(inner):
                decay = decay_ref[pl.ds(pair * inner + head, 1), :]
                decay_here = decay[:, here]
                query_decay = jnp.sum(
                    jnp.where(row == col, decay_here, 0.0), axis=1, keepdims=True
                )
                near = scores_of(query_block, k_head[head, here, :])
                near = near + (query_decay - decay_here)
                near = jnp.where(col <= row, near, -jnp.inf)
                highest = jnp.max(near, axis=1, keepdims=True)
                if block > 0:
                    far = scores_of(query_block, k_head[head, :first, :])
                    far = far + (query_decay - decay[:, :first])
                    highest = jnp.maximum(highest, jnp.max(far, axis=1, keepdims=True))
                total = jnp.dot(
                    jnp.exp(near - highest).astype(jnp.bfloat16),
                    v_ones[here, :],
                    preferred_element_type=jnp.float32,
                )
                if block > 0:
                    total = total + jnp.dot(
                        jnp.exp(far - highest).astype(jnp.bfloat16),
                        v_ones[:first, :],
                        preferred_element_type=jnp.float32,
                    )
                result = total[:, :LANES] / total[:, LANES:]
                merged = result if head == 0 else jnp.where(out_lane == head, result, merged)
            o_buf[pair, here, :] = merged.astype(jnp.bfloat16)
        for step in range(1, n):
            backward(pair, step).start()
        own_back(pair).start()
        return carry

    lax.fori_loop(0, pairs, one_pair, 0)

    def finish(pair, carry):
        own_back(pair).wait()
        for step in range(1, n):
            backward(pair, step).wait()
            for kind in range(3):
                outgoing(kind, pair, step).wait_send()
        return carry

    lax.fori_loop(0, pairs, finish, 0)


def exchange_attention(queries, keys, values, decay, query_gain, key_gain):
    tok, width = queries.shape
    n = lax.axis_size("sp")
    head_size = query_gain.shape[0]
    inner = LANES // head_size
    pairs = width // n // LANES
    length = n * tok
    return pl.pallas_call(
        functools.partial(attention_kernel, n, head_size),
        out_shape=jax.ShapeDtypeStruct((tok, width), jnp.bfloat16),
        in_specs=[pl.BlockSpec(memory_space=pltpu.VMEM)] * 6,
        out_specs=pl.BlockSpec(memory_space=pltpu.VMEM),
        scratch_shapes=[
            pltpu.VMEM((pairs, length, LANES), jnp.bfloat16),
            pltpu.VMEM((pairs, length, LANES), jnp.bfloat16),
            pltpu.VMEM((pairs, length, LANES), jnp.bfloat16),
            pltpu.VMEM((length, LANES), jnp.bfloat16),
            pltpu.VMEM((inner, length, LANES), jnp.bfloat16),
            pltpu.VMEM((length, 2 * LANES), jnp.bfloat16),
            pltpu.VMEM((pairs, length, LANES), jnp.bfloat16),
            pltpu.SemaphoreType.DMA((3, pairs)),
            pltpu.SemaphoreType.DMA((3, pairs, n)),
            pltpu.SemaphoreType.DMA((3, pairs, n)),
            pltpu.SemaphoreType.DMA((pairs,)),
            pltpu.SemaphoreType.DMA((pairs, n)),
            pltpu.SemaphoreType.DMA((pairs, n)),
        ],
        compiler_params=pltpu.CompilerParams(
            collective_id=0, has_side_effects=True, vmem_limit_bytes=40 * 1024 * 1024
        ),
        name="attention",
    )(
        queries, keys, values, decay,
        jnp.tile(query_gain, inner)[None, :], jnp.tile(key_gain, inner)[None, :],
    )


def expert_kernel(
    sp_size, dp_size, per,
    send_ref, gate_ref, up_ref, down_ref,
    out_ref,
    arrived, result, gate_buf, up_buf, down_buf,
    weight_sem, send_sem, recv_sem, back_send, back_recv,
):
    n = sp_size * dp_size
    me = lax.axis_index("sp") * dp_size + lax.axis_index("dp")
    cap, width = send_ref.shape[1], send_ref.shape[2]
    loads = [
        pltpu.make_async_copy(source, target, weight_sem.at[index])
        for index, (source, target) in enumerate(
            ((gate_ref, gate_buf), (up_ref, up_buf), (down_ref, down_buf))
        )
    ]
    for load in loads:
        load.start()

    def coords(flat):
        return {"sp": flat // dp_size, "dp": flat % dp_size}

    barrier = pltpu.get_barrier_semaphore()

    def greet(step, carry):
        pl.semaphore_signal(
            barrier, inc=1, device_id=coords((me + step) % n), device_id_type=MESH
        )
        return carry

    lax.fori_loop(1, n, greet, 0)
    pl.semaphore_wait(barrier, n - 1)

    def outgoing(step):
        target = (me + step) % n
        return pltpu.make_async_remote_copy(
            src_ref=send_ref.at[target],
            dst_ref=arrived.at[step],
            send_sem=send_sem.at[step],
            recv_sem=recv_sem.at[step],
            device_id=coords(target),
            device_id_type=MESH,
        )

    def backward(step):
        target = (me + n - step) % n
        return pltpu.make_async_remote_copy(
            src_ref=result.at[step],
            dst_ref=out_ref.at[me],
            send_sem=back_send.at[step],
            recv_sem=back_recv.at[step],
            device_id=coords(target),
            device_id_type=MESH,
        )

    own = pltpu.make_async_copy(send_ref.at[me], arrived.at[0], recv_sem.at[0])
    own_back = pltpu.make_async_copy(result.at[0], out_ref.at[me], back_recv.at[0])

    def launch(step, carry):
        outgoing(step).start()
        return carry

    lax.fori_loop(1, n, launch, 0)
    own.start()
    for load in loads:
        load.wait()

    def chunk(index, carry):
        first = index * per
        for offset in range(per):
            if offset == 0:
                @pl.when(index == 0)
                def _():
                    own.wait()

                @pl.when(index > 0)
                def _():
                    outgoing(first).wait_recv()
            else:
                outgoing(first + offset).wait_recv()
        rows = arrived[pl.ds(first, per)].reshape(per * cap, width)
        gate = jnp.dot(rows, gate_buf[...], preferred_element_type=jnp.float32)
        upper = jnp.dot(rows, up_buf[...], preferred_element_type=jnp.float32)
        hidden = (gate / (1.0 + jnp.exp(-gate)) * upper).astype(jnp.bfloat16)
        product = jnp.dot(hidden, down_buf[...], preferred_element_type=jnp.float32)
        result[pl.ds(first, per)] = product.astype(jnp.bfloat16).reshape(per, cap, width)
        for offset in range(per):
            if offset == 0:
                @pl.when(index == 0)
                def _():
                    own_back.start()

                @pl.when(index > 0)
                def _():
                    backward(first).start()
            else:
                backward(first + offset).start()
        return carry

    lax.fori_loop(0, n // per, chunk, 0)

    def finish(step, carry):
        outgoing(step).wait_send()
        backward(step).wait()
        return carry

    own_back.wait()
    lax.fori_loop(1, n, finish, 0)


def run_experts(send, gate, upper, down):
    n, cap, width = send.shape
    sp_size, dp_size = lax.axis_size("sp"), lax.axis_size("dp")
    per = max(1, min(n, LANES // cap))
    return pl.pallas_call(
        functools.partial(expert_kernel, sp_size, dp_size, per),
        out_shape=jax.ShapeDtypeStruct(send.shape, jnp.bfloat16),
        in_specs=[pl.BlockSpec(memory_space=pltpu.VMEM)]
        + [pl.BlockSpec(memory_space=pl.ANY)] * 3,
        out_specs=pl.BlockSpec(memory_space=pltpu.VMEM),
        scratch_shapes=[
            pltpu.VMEM(send.shape, jnp.bfloat16),
            pltpu.VMEM(send.shape, jnp.bfloat16),
            pltpu.VMEM(gate.shape, jnp.bfloat16),
            pltpu.VMEM(upper.shape, jnp.bfloat16),
            pltpu.VMEM(down.shape, jnp.bfloat16),
            pltpu.SemaphoreType.DMA((3,)),
            pltpu.SemaphoreType.DMA((n,)),
            pltpu.SemaphoreType.DMA((n,)),
            pltpu.SemaphoreType.DMA((n,)),
            pltpu.SemaphoreType.DMA((n,)),
        ],
        compiler_params=pltpu.CompilerParams(
            collective_id=1, has_side_effects=True, vmem_limit_bytes=56 * 1024 * 1024
        ),
        name="experts",
    )(send, gate, upper, down)


def shards(
    resid,
    queries,
    keys,
    values,
    forget_cache,
    query_gain,
    key_gain,
    out_weight,
    norm_gain,
    routes,
    group_weight,
    inner_share,
    expert_gate,
    expert_up,
    expert_down,
):
    token_attn = exchange_attention(
        queries[0], keys[0], values[0], forget_cache[0], query_gain, key_gain
    )
    projected = jnp.dot(
        token_attn,
        lax.all_gather(out_weight, "dp", axis=1, tiled=True),
        preferred_element_type=jnp.float32,
    )
    mid = (resid[0].astype(jnp.float32) + projected).astype(jnp.bfloat16)
    normed = norm_rows(mid, norm_gain)
    width = normed.shape[1]
    tok_count = normed.shape[0]
    top_count = routes.shape[2]
    experts = lax.axis_size("sp") * lax.axis_size("dp")
    capacity = 2 * tok_count * top_count // experts
    expert_ids = routes[0].reshape(-1)
    expert_onehot = (expert_ids[:, None] == jnp.arange(experts, dtype=jnp.int32)[None, :]).astype(
        jnp.int32
    )
    earlier = jnp.cumsum(expert_onehot, axis=0) - expert_onehot
    slot_rank = jnp.sum(earlier * expert_onehot, axis=1)
    slot_index = (expert_ids * capacity + slot_rank).reshape(tok_count, top_count)
    slot_range = jnp.arange(experts * capacity, dtype=jnp.int32)
    dispatch = jnp.any(slot_range[:, None, None] == slot_index[None, :, :], axis=2).astype(
        jnp.bfloat16
    )
    send = jnp.dot(dispatch, normed, preferred_element_type=jnp.float32).astype(jnp.bfloat16)
    returned = run_experts(
        send.reshape(experts, capacity, width), expert_gate[0], expert_up[0], expert_down[0]
    )
    returned = returned.reshape(experts * capacity, width)
    shares = inner_share[0]
    weights = group_weight[0][:, None] * shares / jnp.sum(shares, axis=-1, keepdims=True)
    mixed = jnp.zeros((tok_count, width), jnp.float32)
    for route in range(top_count):
        select = (slot_range[None, :] == slot_index[:, route : route + 1]).astype(jnp.bfloat16)
        picked = jnp.dot(select, returned, preferred_element_type=jnp.float32)
        mixed = mixed + weights[:, route : route + 1] * picked
    layer_out = (mid.astype(jnp.float32) + mixed).astype(jnp.bfloat16)
    return layer_out.reshape(1, tok_count, width)


def solution(mesh):
    return jax.shard_map(
        shards,
        mesh=mesh,
        in_specs=(
            P("dp", "sp", None),
            P("dp", "sp", None),
            P("dp", "sp", None),
            P("dp", "sp", None),
            P("dp", "sp", None),
            P(),
            P(),
            P(None, "dp"),
            P(),
            P("dp", "sp", None),
            P("dp", "sp"),
            P("dp", "sp", None),
            P(("sp", "dp"), None, None),
            P(("sp", "dp"), None, None),
            P(("sp", "dp"), None, None),
        ),
        out_specs=P("dp", "sp", None),
        check_vma=False,
    )
```

profile of v0, /device:TPU:0, one launch (start us, length us, event | category | flops | bytes accessed | tf_op | source)
XLA Modules:
  0.0 200.9 jit_solution(960392968907406530)
XLA Ops:
  6.5 0.0 copy-start.8
  6.5 0.0 copy-start.10
  6.5 0.0 copy-start.11
  6.5 0.0 copy-start.7
  6.5 0.0 copy-start
  6.5 0.0 copy-start.1
  6.6 0.0 copy-start.2
  6.6 0.0 copy-start.3
  6.6 0.0 all-gather.2.cloned.1.call-start
  6.6 0.7 all-gather.2.cloned.1.call-update
  7.3 0.0 copy-done.8
  7.3 0.0 copy-start.9
  7.3 0.0 copy-start.5
  7.3 0.1 copy.25
  7.5 0.1 eq.71
  7.6 0.1 eq.75
  7.8 0.6 reduce-window.6
  8.3 0.2 slice_reduce_fusion.2
  8.6 0.1 fusion.13
  8.7 0.1 reduce_sum.34
  8.8 0.1 reduce_sum.33
  9.0 0.0 copy-done.10
  9.0 0.1 broadcast_in_dim_tile.6.q_gain_ref
  9.1 0.0 copy-done.11
  9.1 0.1 broadcast_in_dim_tile.7.k_gain_ref
  9.2 0.1 copy.29
  9.2 0.0 copy-done.7
  9.3 0.0 copy-done
  9.3 0.0 copy-done.1
  9.3 0.0 copy-done.2
  9.3 0.0 copy-done.3
  9.3 57.3 %attention.1 = bf16[128,2048]{1,0:T(8,128)(2,1)S(1)} custom-call(bf16[128,2048]{1,0:T(8,128)(2,1)S(1)} %bitcast.51, bf16[128,2048]{1,0:T(8,128)(2,1)S(1)} %bitcast.52, bf16[128,2048]{1,0:T(8,128)(2,1)S(1)} %bitcast.53, f32[4,1024]{1,0:T(4,128)S(1)} %bitcast.54, f32[1,128]{1,0:T(1,128)S(1)} %broadcast_in_dim_tile.6.q_gain_ref, ...), custom_call_target="tpu_custom_call" | custom-call | tf_op jit(solution)/shard_map/attention/pallas_call | solution.py:187
  66.6 0.2 slice_reduce_fusion
  66.8 0.1 fusion.8
  66.8 0.0 copy-done.9
  66.9 0.0 copy-start.6
  66.9 3.1 %all-gather.2.cloned.1.call-done = bf16[2048,2048]{1,0:T(8,128)(2,1)} async-done(((bf16[2048,512]{1,0:T(8,128)(2,1)}), bf16[2048,2048]{1,0:T(8,128)(2,1)}) %all-gather.2.cloned.1.call-update) | async-done | bytes 8388624 | tf_op jit(solution)/shard_map/all_gather | solution.py:378
  70.0 0.0 copy-done.5
  70.0 4.8 %multiply_reduce_fusion = (f32[128]{0:T(128)S(1)}, f32[128,2048]{1,0:T(8,128)S(1)}) fusion(bf16[128,2048]{1,0:T(8,128)(2,1)S(1)} %attention.1, bf16[2048,2048]{1,0:T(8,128)(2,1)} %all-gather.2.cloned.1.call-done, bf16[1,128,2048]{2,1,0:T(8,128)(2,1)S(1)} %copy-done.5), kind=kOutput, calls=%fused_computation.11 | convolution fusion | flops 1075314560 | bytes 10486272 | tf_op jit(solution)/shard_map/dot_general | solution.py:376
  74.8 0.0 copy-done.6
  74.8 2.1 %convolution_convert_fusion = bf16[512,2048]{1,0:T(8,128)(2,1)} fusion(pred[512,128]{1,0:T(8,128)(4,1)S(1)} %fusion.8, f32[128,2048]{1,0:T(8,128)S(1)} %get-tuple-element.10, f32[2048]{0:T(1024)S(1)} %copy-done.6, f32[128]{0:T(128)S(1)} %add_rsqrt_fusion), kind=kOutput, calls=%fused_computation | convolution fusion | flops 270270464 | bytes 3219968 | tf_op jit(solution)/shard_map/dot_general | solution.py:399
  77.0 113.5 %experts.1 = bf16[32,16,2048]{2,1,0:T(8,128)(2,1)} custom-call(bf16[32,16,2048]{2,1,0:T(8,128)(2,1)} %bitcast.57, bf16[2048,1024]{1,0:T(8,128)(2,1)} %bitcast.58, bf16[2048,1024]{1,0:T(8,128)(2,1)} %bitcast.59, bf16[1024,2048]{1,0:T(8,128)(2,1)} %bitcast.60), custom_call_target="tpu_custom_call" | custom-call | tf_op jit(solution)/shard_map/experts/pallas_call | solution.py:331
  190.5 0.0 copy-start.4
  190.5 2.2 %convolution_multiply_fusion.1 = f32[128,2048]{1,0:T(8,128)S(1)} fusion(bf16[512,2048]{1,0:T(8,128)(2,1)} %bitcast.55, f32[128]{0:T(128)S(1)} %get-tuple-element.8, s32[128]{0:T(128)S(1)} %get-tuple-element.6), kind=kOutput, calls=%fused_computation.4 | convolution fusion | flops 268763136 | bytes 3146752 | tf_op jit(solution)/shard_map/dot_general | solution.py:409
  192.7 0.0 copy-done.4
  192.7 1.4 fusion.5
  (11 shorter events, 0.1 us)
Async XLA Ops:
  6.5 0.8 copy-start.8
  6.5 2.4 %copy-start.10 = (f32[64]{0:T(128)S(1)}, f32[64]{0:T(128)}, u32[]{:S(2)}) copy-start(f32[64]{0:T(128)} %param.20) | copy-start | bytes 772
  6.5 2.5 %copy-start.11 = (f32[64]{0:T(128)S(1)}, f32[64]{0:T(128)}, u32[]{:S(2)}) copy-start(f32[64]{0:T(128)} %param.21) | copy-start | bytes 772
  6.5 2.7 %copy-start.7 = (f32[1,128,2]{1,2,0:T(2,128)S(1)}, f32[1,128,2]{1,2,0:T(2,128)}, u32[]{:S(2)}) copy-start(f32[1,128,2]{1,2,0:T(2,128)} %param.26) | copy-start | bytes 3076
  6.5 2.7 %copy-start = (bf16[1,128,2048]{2,1,0:T(8,128)(2,1)S(1)}, bf16[1,128,2048]{2,1,0:T(8,128)(2,1)}, u32[]{:S(2)}) copy-start(bf16[1,128,2048]{2,1,0:T(8,128)(2,1)} %param.16) | copy-start | bytes 1572868
  6.5 2.7 %copy-start.1 = (bf16[1,128,2048]{2,1,0:T(8,128)(2,1)S(1)}, bf16[1,128,2048]{2,1,0:T(8,128)(2,1)}, u32[]{:S(2)}) copy-start(bf16[1,128,2048]{2,1,0:T(8,128)(2,1)} %param.17) | copy-start | bytes 1572868
  6.6 2.7 %copy-start.2 = (bf16[1,128,2048]{2,1,0:T(8,128)(2,1)S(1)}, bf16[1,128,2048]{2,1,0:T(8,128)(2,1)}, u32[]{:S(2)}) copy-start(bf16[1,128,2048]{2,1,0:T(8,128)(2,1)} %param.18) | copy-start | bytes 1572868
  6.6 2.7 %copy-start.3 = (f32[1,4,1024]{2,1,0:T(4,128)S(1)}, f32[1,4,1024]{2,1,0:T(4,128)}, u32[]{:S(2)}) copy-start(f32[1,4,1024]{2,1,0:T(4,128)} %param.19) | copy-start | bytes 49156
  6.6 63.4 %all-gather.2.cloned.1.call-start = ((), (), s32[]{:S(2)}) async-start(), calls=%async_computation | async-start | bytes 10485760 | tf_op jit(solution)/shard_map/all_gather | solution.py:378
  7.3 59.5 %copy-start.9 = (f32[1,128]{1,0:T(1,128)S(1)}, f32[1,128]{1,0:T(1,128)}, u32[]{:S(2)}) copy-start(f32[1,128]{1,0:T(1,128)} %param.25) | copy-start | bytes 1540
  7.3 62.6 %copy-start.5 = (bf16[1,128,2048]{2,1,0:T(8,128)(2,1)S(1)}, bf16[1,128,2048]{2,1,0:T(8,128)(2,1)}, u32[]{:S(2)}) copy-start(bf16[1,128,2048]{2,1,0:T(8,128)(2,1)} %param.15) | copy-start | bytes 1572868
  66.9 7.9 %copy-start.6 = (f32[2048]{0:T(1024)S(1)}, f32[2048]{0:T(1024)}, u32[]{:S(2)}) copy-start(f32[2048]{0:T(1024)} %param.23) | copy-start | bytes 24580
  190.5 2.2 %copy-start.4 = (bf16[32,16,2048]{2,1,0:T(8,128)(2,1)S(1)}, bf16[32,16,2048]{2,1,0:T(8,128)(2,1)}, u32[]{:S(2)}) copy-start(bf16[32,16,2048]{2,1,0:T(8,128)(2,1)} %experts.1) | copy-start | bytes 6291460
Sparse Core Ops, SparseCore 0:
  8.9 60.9 all-gather.1
where the time goes:
time: 201 us
  Pallas kernels  171 us (85%)
  between operations  13.6 us (7%)
  matrix products  10.6 us (5%)
  waiting for transfers between devices  3.75 us (2%)
    pallas_call x1, Pallas kernels, run_experts(): pl.pallas_call(functools.partial(expert_kernel, sp_size, dp_size, per), o...  113 us
    pallas_call x1, Pallas kernels, exchange_attention(): pl.pallas_call(functools.partial(attention_kernel, n, head_size), out_sha...  57.3 us
    dot_general x1, matrix products, shards(): jnp.dot(token_attn, lax.all_gather(out_weight, 'dp', axis=1, tiled=True),...  4.83 us
  transfers between devices with their start and end apart: 1, of which 1 were waited for; matrix products, arithmetic and copies ran while one was open for 1% of the time, Pallas kernels for 29%

commit v1 on v0

--- a/solution.py
+++ b/solution.py
@@ -37,13 +37,18 @@
 
 
 def attention_kernel(
-    n, head_size,
-    q_ref, k_ref, v_ref, decay_ref, q_gain_ref, k_gain_ref,
-    out_ref,
+    n, dp_size, head_size,
+    q_ref, k_ref, v_ref, decay_ref, q_gain_ref, k_gain_ref, weight_ref,
+    projected_ref, out_ref, weights,
     q_buf, k_buf, v_buf, q_norm, k_head, v_ones, o_buf,
     local_sem, send_sem, recv_sem, own_sem, back_send, back_recv,
+    weight_sem, weight_send, weight_recv, pass_send, pass_recv,
 ):
     me = lax.axis_index("sp")
+    column = lax.axis_index("dp")
+    rows_y = dp_size // 2
+    row_y, core = column // 2, column % 2
+    twin = row_y * 2 + 1 - core
     tok = q_ref.shape[0]
     pairs, length = q_buf.shape[0], q_buf.shape[1]
     inner = LANES // head_size
@@ -54,7 +59,36 @@
         pl.semaphore_signal(
             barrier, inc=1, device_id={"sp": lax.rem(me + step, n)}, device_id_type=MESH
         )
-    pl.semaphore_wait(barrier, n - 1)
+    for step in range(1, rows_y):
+        pl.semaphore_signal(
+            barrier, inc=1, device_id={"dp": lax.rem(row_y + step, rows_y) * 2 + core},
+            device_id_type=MESH,
+        )
+    pl.semaphore_signal(barrier, inc=1, device_id={"dp": twin}, device_id_type=MESH)
+    pl.semaphore_wait(barrier, n - 1 + rows_y)
+
+    def weight_across(step):
+        return pltpu.make_async_remote_copy(
+            src_ref=weight_ref,
+            dst_ref=weights.at[column],
+            send_sem=weight_send.at[step],
+            recv_sem=weight_recv.at[step],
+            device_id={"dp": lax.rem(row_y + step, rows_y) * 2 + core},
+            device_id_type=MESH,
+        )
+
+    def weight_pass(step):
+        block = lax.rem(row_y + rows_y - step, rows_y) * 2 + core
+        return pltpu.make_async_remote_copy(
+            src_ref=weight_ref if step == 0 else weights.at[block],
+            dst_ref=weights.at[block],
+            send_sem=pass_send.at[step],
+            recv_sem=pass_recv.at[step],
+            device_id={"dp": twin},
+            device_id_type=MESH,
+        )
+
+    weight_own = pltpu.make_async_copy(weight_ref, weights.at[column], weight_sem)
 
     def outgoing(kind, pair, step):
         target = lax.rem(me + step, n)
@@ -98,6 +132,11 @@
                 outgoing(kind, pair, step).start()
         for kind in range(3):
             own(kind, pair).start()
+
+    for step in range(1, rows_y):
+        weight_across(step).start()
+    weight_pass(0).start()
+    weight_own.start()
 
     row = lax.broadcasted_iota(jnp.int32, (BLOCK, BLOCK), 0)
     col = lax.broadcasted_iota(jnp.int32, (BLOCK, BLOCK), 1)
@@ -165,6 +204,9 @@
         return carry
 
     lax.fori_loop(0, pairs, one_pair, 0)
+    for step in range(1, rows_y):
+        weight_across(step).wait_recv()
+        weight_pass(step).start()
 
     def finish(pair, carry):
         own_back(pair).wait()
@@ -175,21 +217,34 @@
         return carry
 
     lax.fori_loop(0, pairs, finish, 0)
-
-
-def exchange_attention(queries, keys, values, decay, query_gain, key_gain):
+    weight_own.wait()
+    for step in range(1, rows_y):
+        weight_across(step).wait_send()
+    for step in range(rows_y):
+        weight_pass(step).wait()
+    span = weights.shape[2]
+    for block in range(dp_size):
+        projected_ref[:, block * span : (block + 1) * span] = jnp.dot(
+            out_ref[...], weights[block], preferred_element_type=jnp.float32
+        )
+
+
+def exchange_attention(queries, keys, values, decay, query_gain, key_gain, out_weight):
     tok, width = queries.shape
-    n = lax.axis_size("sp")
+    n, dp_size = lax.axis_size("sp"), lax.axis_size("dp")
     head_size = query_gain.shape[0]
     inner = LANES // head_size
     pairs = width // n // LANES
     length = n * tok
     return pl.pallas_call(
-        functools.partial(attention_kernel, n, head_size),
-        out_shape=jax.ShapeDtypeStruct((tok, width), jnp.bfloat16),
-        in_specs=[pl.BlockSpec(memory_space=pltpu.VMEM)] * 6,
+        functools.partial(attention_kernel, n, dp_size, head_size),
+        out_shape=jax.ShapeDtypeStruct((tok, dp_size * out_weight.shape[1]), jnp.float32),
+        in_specs=[pl.BlockSpec(memory_space=pltpu.VMEM)] * 6
+        + [pl.BlockSpec(memory_space=pl.ANY)],
         out_specs=pl.BlockSpec(memory_space=pltpu.VMEM),
         scratch_shapes=[
+            pltpu.VMEM((tok, width), jnp.bfloat16),
+            pltpu.VMEM((dp_size,) + out_weight.shape, jnp.bfloat16),
             pltpu.VMEM((pairs, length, LANES), jnp.bfloat16),
             pltpu.VMEM((pairs, length, LANES), jnp.bfloat16),
             pltpu.VMEM((pairs, length, LANES), jnp.bfloat16),
@@ -203,6 +258,11 @@
             pltpu.SemaphoreType.DMA((pairs,)),
             pltpu.SemaphoreType.DMA((pairs, n)),
             pltpu.SemaphoreType.DMA((pairs, n)),
+            pltpu.SemaphoreType.DMA,
+            pltpu.SemaphoreType.DMA((dp_size,)),
+            pltpu.SemaphoreType.DMA((dp_size,)),
+            pltpu.SemaphoreType.DMA((dp_size,)),
+            pltpu.SemaphoreType.DMA((dp_size,)),
         ],
         compiler_params=pltpu.CompilerParams(
             collective_id=0, has_side_effects=True, vmem_limit_bytes=40 * 1024 * 1024
@@ -211,6 +271,7 @@
     )(
         queries, keys, values, decay,
         jnp.tile(query_gain, inner)[None, :], jnp.tile(key_gain, inner)[None, :],
+        out_weight,
     )
 
 
@@ -223,6 +284,17 @@
 ):
     n = sp_size * dp_size
     me = lax.axis_index("sp") * dp_size + lax.axis_index("dp")
+    layers = 4 if sp_size % 4 == 0 else 1
+    plane = n // layers
+    layer, seat = me // plane, me % plane
+
+    def partner(step, sign):
+        group, turn = step // plane, step % plane
+        high = (layer // 2 + 1 - group // 2) % 2
+        low = (layer + (group + 1) // 2) % 2
+        other = 2 * high + low if layers == 4 else layer
+        return other * plane + (seat + plane + sign * turn) % plane
+
     cap, width = send_ref.shape[1], send_ref.shape[2]
     loads = [
         pltpu.make_async_copy(source, target, weight_sem.at[index])
@@ -248,7 +320,7 @@
     pl.semaphore_wait(barrier, n - 1)
 
     def outgoing(step):
-        target = (me + step) % n
+        target = partner(step, 1)
         return pltpu.make_async_remote_copy(
             src_ref=send_ref.at[target],
             dst_ref=arrived.at[step],
@@ -259,7 +331,7 @@
         )
 
     def backward(step):
-        target = (me + n - step) % n
+        target = partner(step, -1)
         return pltpu.make_async_remote_copy(
             src_ref=result.at[step],
             dst_ref=out_ref.at[me],
@@ -269,14 +341,16 @@
             device_id_type=MESH,
         )
 
-    own = pltpu.make_async_copy(send_ref.at[me], arrived.at[0], recv_sem.at[0])
-    own_back = pltpu.make_async_copy(result.at[0], out_ref.at[me], back_recv.at[0])
+    mine = n - plane
+    own = pltpu.make_async_copy(send_ref.at[me], arrived.at[mine], recv_sem.at[mine])
+    own_back = pltpu.make_async_copy(result.at[mine], out_ref.at[me], back_recv.at[mine])
 
     def launch(step, carry):
         outgoing(step).start()
         return carry
 
-    lax.fori_loop(1, n, launch, 0)
+    lax.fori_loop(0, mine, launch, 0)
+    lax.fori_loop(mine + 1, n, launch, 0)
     own.start()
     for load in loads:
         load.wait()
@@ -285,11 +359,11 @@
         first = index * per
         for offset in range(per):
             if offset == 0:
-                @pl.when(index == 0)
+                @pl.when(first == mine)
                 def _():
                     own.wait()
 
-                @pl.when(index > 0)
+                @pl.when(first != mine)
                 def _():
                     outgoing(first).wait_recv()
             else:
@@ -302,11 +376,11 @@
         result[pl.ds(first, per)] = product.astype(jnp.bfloat16).reshape(per, cap, width)
         for offset in range(per):
             if offset == 0:
-                @pl.when(index == 0)
+                @pl.when(first == mine)
                 def _():
                     own_back.start()
 
-                @pl.when(index > 0)
+                @pl.when(first != mine)
                 def _():
                     backward(first).start()
             else:
@@ -321,7 +395,8 @@
         return carry
 
     own_back.wait()
-    lax.fori_loop(1, n, finish, 0)
+    lax.fori_loop(0, mine, finish, 0)
+    lax.fori_loop(mine + 1, n, finish, 0)
 
 
 def run_experts(send, gate, upper, down):
@@ -370,13 +445,8 @@
     expert_up,
     expert_down,
 ):
-    token_attn = exchange_attention(
-        queries[0], keys[0], values[0], forget_cache[0], query_gain, key_gain
-    )
-    projected = jnp.dot(
-        token_attn,
-        lax.all_gather(out_weight, "dp", axis=1, tiled=True),
-        preferred_element_type=jnp.float32,
+    projected = exchange_attention(
+        queries[0], keys[0], values[0], forget_cache[0], query_gain, key_gain, out_weight
     )
     mid = (resid[0].astype(jnp.float32) + projected).astype(jnp.bfloat16)
     normed = norm_rows(mid, norm_gain)

time: 201 us -> 177 us (0.88)
  between operations: 13.6 us -> 0.14 us
  Pallas kernels: 171 us -> 159 us
  local copies, waits for them, and re-layouts: 1.32 us -> 9.12 us
  matrix products: 10.6 us -> 5.71 us
  waiting for transfers between devices: 3.75 us -> 0 us
    pallas_call x1, Pallas kernels: 113 us -> 99.9 us  [run_experts(): pl.pallas_call(functools.partial(expert_kernel, sp_size, dp_size, per), o...]
    unnamed x25 -> x17, local copies, waits for them, and re-layouts: 0.16 us -> 6.65 us
    dot_general x1 -> x0, matrix products: 4.83 us -> none  [shards(): jnp.dot(token_attn, lax.all_gather(out_weight, 'dp', axis=1, tiled=True),...]
    all_gather x1 -> x0, waiting for transfers between devices: 3.07 us -> none  [shards(): lax.all_gather(out_weight, 'dp', axis=1, tiled=True)]
    pallas_call x1, Pallas kernels: 57.3 us -> 59.5 us  [exchange_attention(): pl.pallas_call(functools.partial(attention_kernel, n, dp_size, head_size)...]
  transfers between devices with their start and end apart: 1 -> 0, of which waited for: 1 -> 0; matrix products, arithmetic and copies ran while one was open for 1% -> 0% of each run, Pallas kernels for 29% -> 0%
where the time goes in v1:
time: 177 us
  Pallas kernels  159 us (90%)
  local copies, waits for them, and re-layouts  9.12 us (5%)
  matrix products  5.71 us (3%)
  other arithmetic  2.48 us (1%)
    pallas_call x1, Pallas kernels, run_experts(): pl.pallas_call(functools.partial(expert_kernel, sp_size, dp_size, per), o...  99.9 us
    pallas_call x1, Pallas kernels, exchange_attention(): pl.pallas_call(functools.partial(attention_kernel, n, dp_size, head_size)...  59.5 us
    unnamed x17, local copies, waits for them, and re-layouts  6.65 us
    dot_general x2, matrix products, shards(): picked = jnp.dot(select, returned, preferred_element_type=jnp.float32)  3.58 us

profile of v1, /device:TPU:0, one launch (start us, length us, event | category | flops | bytes accessed | tf_op | source)
XLA Modules:
  0.0 176.9 jit_solution(1797798232868527673)
XLA Ops:
  0.0 0.7 reduce_sum.31
  0.7 0.7 fusion.18
  1.4 0.7 tile.4
  2.0 0.1 broadcast_in_dim_tile.6.q_gain_ref
  2.1 0.7 tile.5
  2.8 0.1 broadcast_in_dim_tile.7.k_gain_ref
  2.9 0.8 copy.25
  3.7 0.1 eq.75
  3.8 0.1 eq.71
  4.0 0.6 reduce-window.6
  4.5 0.2 slice_reduce_fusion.2
  4.8 0.1 fusion.16
  4.9 0.1 reduce_sum.34
  5.0 0.1 copy.29
  5.1 0.1 fusion.11
  5.2 0.1 reduce_sum.33
  5.4 0.2 slice_reduce_fusion
  5.5 0.0 copy-start
  5.5 1.6 copy-done
  7.1 0.0 copy-start.1
  7.1 1.0 copy-done.1
  8.2 0.0 copy-start.2
  8.2 1.0 copy-done.2
  9.2 0.0 copy-start.3
  9.2 1.0 copy-done.3
  10.3 0.0 copy-start.4
  10.3 0.7 copy-done.4
  11.0 0.0 copy-start.6
  11.0 59.5 %attention.1 = f32[128,2048]{1,0:T(8,128)S(1)} custom-call(bf16[128,2048]{1,0:T(8,128)(2,1)S(1)} %bitcast.50, bf16[128,2048]{1,0:T(8,128)(2,1)S(1)} %bitcast.51, bf16[128,2048]{1,0:T(8,128)(2,1)S(1)} %bitcast.52, f32[4,1024]{1,0:T(4,128)S(1)} %bitcast.53, f32[1,128]{1,0:T(1,128)S(1)} %broadcast_in_dim_tile.6.q_gain_ref, ...), custom_call_target="tpu_custom_call" | custom-call | tf_op jit(solution)/shard_map/attention/pallas_call | solution.py:239
  70.5 0.0 copy-done.6
  70.5 0.0 copy-start.7
  70.5 0.3 fusion.4
  70.8 0.4 copy-done.7
  71.2 2.1 %convolution_convert_fusion = bf16[512,2048]{1,0:T(8,128)(2,1)} fusion(pred[512,128]{1,0:T(8,128)(4,1)S(1)} %fusion.11, bf16[128,2048]{1,0:T(8,128)(2,1)S(1)} %get-tuple-element.8, f32[2048]{0:T(1024)S(1)} %copy-done.7, f32[128]{0:T(128)S(1)} %add_rsqrt_fusion), kind=kOutput, calls=%fused_computation | convolution fusion | flops 270532608 | bytes 2695680 | tf_op jit(solution)/shard_map/dot_general | solution.py:469
  73.4 99.9 %experts.1 = bf16[32,16,2048]{2,1,0:T(8,128)(2,1)} custom-call(bf16[32,16,2048]{2,1,0:T(8,128)(2,1)} %bitcast.56, bf16[2048,1024]{1,0:T(8,128)(2,1)} %bitcast.57, bf16[2048,1024]{1,0:T(8,128)(2,1)} %bitcast.58, bf16[1024,2048]{1,0:T(8,128)(2,1)} %bitcast.59), custom_call_target="tpu_custom_call" | custom-call | tf_op jit(solution)/shard_map/experts/pallas_call | solution.py:406
  173.3 0.0 copy-start.5
  173.3 2.2 %convolution_multiply_fusion.1 = f32[128,2048]{1,0:T(8,128)S(1)} fusion(bf16[512,2048]{1,0:T(8,128)(2,1)} %bitcast.54, f32[128]{0:T(128)S(1)} %get-tuple-element.10, s32[128]{0:T(128)S(1)} %get-tuple-element.6), kind=kOutput, calls=%fused_computation.4 | convolution fusion | flops 268763136 | bytes 3146752 | tf_op jit(solution)/shard_map/dot_general | solution.py:479
  175.5 0.0 copy-done.5
  175.5 1.4 fusion.3
  (7 shorter events, 0.1 us)
Async XLA Ops:
  5.5 1.6 copy-start
  7.1 1.0 copy-start.1
  8.2 1.0 copy-start.2
  9.2 1.0 copy-start.3
  10.3 0.7 copy-start.4
  11.0 59.5 %copy-start.6 = (bf16[1,128,2048]{2,1,0:T(8,128)(2,1)S(1)}, bf16[1,128,2048]{2,1,0:T(8,128)(2,1)}, u32[]{:S(2)}) copy-start(bf16[1,128,2048]{2,1,0:T(8,128)(2,1)} %param.15) | copy-start | bytes 1572868
  70.5 0.7 copy-start.7
  173.3 2.2 %copy-start.5 = (bf16[32,16,2048]{2,1,0:T(8,128)(2,1)S(1)}, bf16[32,16,2048]{2,1,0:T(8,128)(2,1)}, u32[]{:S(2)}) copy-start(bf16[32,16,2048]{2,1,0:T(8,128)(2,1)} %experts.1) | copy-start | bytes 6291460
